TPU v7x, 32 devices: a whole 2x2x4 slice. The times are simulated.
32 devices in a mesh: tp: 8 (over z, x), dp: 4 (over y, core).
Axes of the slice: x: 2, y: 2, z: 4, core: 2. Of those that a mesh axis runs over, the one named last changes fastest.
Arguments:
- tokens: bfloat16 [128, 4096], P('tp', 'dp'), may hold values from -6 to 6
- query_weight: bfloat16 [2, 4096, 2048], P(None, 'dp', 'tp'), may hold values from -0.09375 to 0.09375
- key_weight: bfloat16 [2, 4096, 2048], P(None, 'dp', 'tp'), may hold values from -0.09375 to 0.09375
- value_weight: bfloat16 [2, 4096, 2048], P(None, 'dp', 'tp'), may hold values from -0.09375 to 0.09375
- outgate_weight: bfloat16 [2, 4096, 2048], P(None, 'dp', 'tp'), may hold values from -0.09375 to 0.09375
- igate_weight: bfloat16 [2, 4096, 16], replicated, may hold values from -0.09375 to 0.09375
- fgate_weight: bfloat16 [2, 4096, 16], replicated, may hold values from -0.09375 to 0.09375
- norm_gain: float32 [2, 4096], P(None, 'dp'), may hold values from 0.1 to 1.9
- head_gain: float32 [2, 2048], P(None, 'tp'), may hold values from 0.1 to 1.9
- proj_weight: bfloat16 [2, 2048, 4096], P(None, 'tp', 'dp'), may hold values from -0.125 to 0.125
- cell_state: float32 [2, 128, 16, 128, 128], P(None, 'dp', 'tp'), may hold values from -1.8 to 1.8
- normer_state: float32 [2, 128, 16, 128], P(None, 'dp', 'tp'), may hold values from -1.8 to 1.8
- stab_state: float32 [2, 128, 16], P(None, 'dp', 'tp'), may hold values from -4 to 4
Outputs:
- final_rows: bfloat16 [128, 4096], P('tp', 'dp')
- cell_out: float32 [2, 128, 16, 128, 128], P(None, 'dp', 'tp')
- normer_out: float32 [2, 128, 16, 128], P(None, 'dp', 'tp')
- stab_out: float32 [2, 128, 16], P(None, 'dp', 'tp')
All inputs are finite; a program needn't handle non-finite values.
Results may differ from a plain program's by a relative error of at most 0.012.
The roundings to bfloat16 on the way count: a program that leaves them out, or rounds other values in their place, can miss the bound.
Values may be sent and summed in bfloat16 or wider, within the bound.
A program may use at most 64 MiB of HBM per device.

v0:
```python
import jax
import jax.numpy as jnp
from jax import lax
from jax.sharding import PartitionSpec as P

D = 4096


EPSILON = 1e-06


def gather_rows(block_input):
    return lax.all_gather(block_input, "tp", axis=0, tiled=True)


def spread_heads(out_part):
    return lax.psum_scatter(out_part, "tp", scatter_dimension=0, tiled=True)


def per_device(
    tokens,
    query_weight,
    key_weight,
    value_weight,
    outgate_weight,
    igate_weight,
    fgate_weight,
    norm_gain,
    head_gain,
    proj_weight,
    cell_state,
    normer_state,
    stab_state,
):
    dp_rank = lax.axis_index("dp")
    tp_rank = lax.axis_index("tp")
    local_seqs = cell_state.shape[1]
    local_heads = cell_state.shape[2]
    head_dim = cell_state.shape[3]
    row_width = query_weight.shape[1]
    num_blocks = query_weight.shape[0]
    gathered = gather_rows(tokens)
    final_rows = tokens
    cell_list = []
    normer_list = []
    stab_list = []
    for layer_num in range(num_blocks):
        as_float = gathered.astype(jnp.float32)
        part_squares = jnp.sum(as_float * as_float, axis=1)
        scaled = (as_float * norm_gain[layer_num]).astype(jnp.bfloat16)

        def product(weight):
            return jnp.dot(scaled, weight, preferred_element_type=jnp.float32)

        gate_start = (dp_rank * row_width, tp_rank * local_heads)
        igate_rows = lax.dynamic_slice(
            igate_weight[layer_num], gate_start, (row_width, local_heads)
        )
        fgate_rows = lax.dynamic_slice(
            fgate_weight[layer_num], gate_start, (row_width, local_heads)
        )
        query_part = product(query_weight[layer_num])
        key_part = product(key_weight[layer_num])
        value_part = product(value_weight[layer_num])
        outgate_part = product(outgate_weight[layer_num])
        igate_part = product(igate_rows)
        forget_part = product(fgate_rows)
        query_sum, key_sum, value_sum, outgate_sum, igate_sum, forget_sum = (
            lax.psum_scatter(query_part, "dp", scatter_dimension=0, tiled=True),
            lax.psum_scatter(key_part, "dp", scatter_dimension=0, tiled=True),
            lax.psum_scatter(value_part, "dp", scatter_dimension=0, tiled=True),
            lax.psum_scatter(outgate_part, "dp", scatter_dimension=0, tiled=True),
            lax.psum_scatter(igate_part, "dp", scatter_dimension=0, tiled=True),
            lax.psum_scatter(forget_part, "dp", scatter_dimension=0, tiled=True),
        )
        total_sq = lax.psum(part_squares, "dp")
        own_sq = lax.dynamic_slice_in_dim(total_sq, dp_rank * local_seqs, local_seqs)
        inv_rms = lax.rsqrt(own_sq / D + EPSILON)[:, None]
        query_rows = (query_sum * inv_rms).reshape(local_seqs, local_heads, head_dim)
        key_rows = (key_sum * inv_rms * head_dim ** (-0.5)).reshape(
            local_seqs, local_heads, head_dim
        )
        value_rows = (value_sum * inv_rms).reshape(local_seqs, local_heads, head_dim)
        outgate = outgate_sum * inv_rms
        igate = igate_sum * inv_rms
        forget = jax.nn.log_sigmoid(forget_sum * inv_rms)
        prev_stab = stab_state[layer_num]
        new_stab = jnp.maximum(forget + prev_stab, igate)
        keep_rate = jnp.exp(forget + prev_stab - new_stab)
        write_rate = jnp.exp(igate - new_stab)
        new_cell = (
            keep_rate[..., None, None] * cell_state[layer_num]
            + write_rate[..., None, None] * value_rows[..., :, None] * key_rows[..., None, :]
        )
        new_normer = (
            keep_rate[..., None] * normer_state[layer_num] + write_rate[..., None] * key_rows
        )
        numerator = jnp.einsum(
            "bhvd,bhd->bhv", new_cell, query_rows, precision=lax.Precision.HIGHEST
        )
        denominator = jnp.maximum(jnp.abs(jnp.sum(new_normer * query_rows, axis=-1)), 1.0)
        readout = numerator / denominator[..., None]
        normed = readout * lax.rsqrt(jnp.mean(readout * readout, axis=-1, keepdims=True) + EPSILON)
        normed = normed * head_gain[layer_num].reshape(local_heads, head_dim)
        gated_out = (
            jax.nn.sigmoid(outgate) * normed.reshape(local_seqs, local_heads * head_dim)
        ).astype(jnp.bfloat16)
        all_gated = lax.all_gather(gated_out, "dp", axis=0, tiled=True)
        out_part = jnp.dot(all_gated, proj_weight[layer_num], preferred_element_type=jnp.float32)
        if layer_num + 1 < num_blocks:
            gathered = lax.psum(out_part, "tp").astype(jnp.bfloat16)
        else:
            final_rows = spread_heads(out_part).astype(jnp.bfloat16)
        cell_list.append(new_cell)
        normer_list.append(new_normer)
        stab_list.append(new_stab)
    return (final_rows, jnp.stack(cell_list), jnp.stack(normer_list), jnp.stack(stab_list))


def solution(mesh):
    return jax.shard_map(
        per_device,
        mesh=mesh,
        in_specs=(
            P("tp", "dp"),
            P(None, "dp", "tp"),
            P(None, "dp", "tp"),
            P(None, "dp", "tp"),
            P(None, "dp", "tp"),
            P(),
            P(),
            P(None, "dp"),
            P(None, "tp"),
            P(None, "tp", "dp"),
            P(None, "dp", "tp", None, None),
            P(None, "dp", "tp", None),
            P(None, "dp", "tp"),
        ),
        out_specs=(
            P("tp", "dp"),
            P(None, "dp", "tp", None, None),
            P(None, "dp", "tp", None),
            P(None, "dp", "tp"),
        ),
        check_vma=False,
    )
```

profile of v0, /device:TPU:0, one launch (start us, length us, event | category | flops | bytes accessed | tf_op | source)
XLA Modules:
  0.0 431.7 jit_solution(14644992044606748619)
XLA Ops:
  8.1 32.8 %all_gather.9 = bf16[128,1024]{1,0:T(8,128)(2,1)S(1)} all-gather(bf16[16,1024]{1,0:T(8,128)(2,1)} %param.13), channel_id=1, replica_groups=mesh['tp'=8,'dp'=4] {'tp'}, dimensions={0}, use_global_device_ids=true | all-gather | bytes 294912 | tf_op jit(solution)/shard_map/all_gather | solution.py:13
  46.1 1.9 fusion.36
  52.3 5.7 %psum.21 = f32[128]{0:T(128)S(1)} all-reduce(f32[128]{0:T(128)S(1)} %fusion.17), channel_id=1, replica_groups=mesh['tp'=8,'dp'=4] {'dp'}, use_global_device_ids=true, to_apply=%region_2.0 | all-reduce | flops 128 | bytes 1024 | tf_op jit(solution)/shard_map/psum | solution.py:76
  58.0 6.2 %reduce-scatter.42.cloned.1.call-done = f32[32,2]{1,0:T(8,128)} async-done(((f32[128,2]{1,0:T(8,128)}), f32[32,2]{1,0:T(8,128)}) %reduce-scatter.42.cloned.1.call-update) | async-done | bytes 272
  65.0 21.2 %reduce-scatter.40.cloned.1.call-done = f32[32,2]{1,0:T(8,128)} async-done(((f32[128,2]{1,0:T(8,128)}), f32[32,2]{1,0:T(8,128)}) %reduce-scatter.40.cloned.1.call-update) | async-done | bytes 272
  87.2 21.6 %reduce-scatter.24.cloned.1.call-done = f32[32,256]{1,0:T(8,128)} async-done(((f32[128,256]{1,0:T(8,128)}), f32[32,256]{1,0:T(8,128)}) %reduce-scatter.24.cloned.1.call-update) | async-done | bytes 32784 | tf_op jit(solution)/shard_map/reduce_scatter | solution.py:71
  108.9 21.9 %reduce-scatter.26.cloned.1.call-done = f32[32,256]{1,0:T(8,128)} async-done(((f32[128,256]{1,0:T(8,128)}), f32[32,256]{1,0:T(8,128)}) %reduce-scatter.26.cloned.1.call-update) | async-done | bytes 32784 | tf_op jit(solution)/shard_map/reduce_scatter | solution.py:70
  130.8 21.9 %reduce-scatter.28.cloned.1.call-done = f32[32,256]{1,0:T(8,128)} async-done(((f32[128,256]{1,0:T(8,128)}), f32[32,256]{1,0:T(8,128)}) %reduce-scatter.28.cloned.1.call-update) | async-done | bytes 32784 | tf_op jit(solution)/shard_map/reduce_scatter | solution.py:69
  153.9 8.6 %fusion.4 = f32[32,2,1,128]{3,2,1,0:T(1,128)S(1)} fusion(f32[32,2,128,1]{2,3,1,0:T(1,128)S(1)} %bitcast.116, f32[2,32,2,128,128]{4,3,2,1,0:T(8,128)} %param.23, f32[32,2,128]{2,1,0:T(2,128)S(1)} %mul.366, f32[32,2,128]{2,1,0:T(2,128)S(1)} %get-tuple-element.25, f32[32,2]{1,0:T(8,128)S(1)} %copy.29), kind=kOutput, calls=%fused_computation.6 | convolution fusion | flops 15728640 | bytes 4325632 | tf_op jit(solution)/shard_map/bhvd,bhd->bhv/dot_general | solution.py:98
  162.8 11.8 %reduce-scatter.22.cloned.1.call-done = f32[32,256]{1,0:T(8,128)} async-done(((f32[128,256]{1,0:T(8,128)}), f32[32,256]{1,0:T(8,128)}) %reduce-scatter.22.cloned.1.call-update) | async-done | bytes 32784 | tf_op jit(solution)/shard_map/reduce_scatter | solution.py:72
  175.5 5.2 %all_gather.10 = bf16[128,256]{1,0:T(8,128)(2,1)S(1)} all-gather(bf16[32,256]{1,0:T(8,128)(2,1)S(1)} %fusion.59), channel_id=1, replica_groups=mesh['tp'=8,'dp'=4] {'dp'}, dimensions={0}, use_global_device_ids=true | all-gather | bytes 81920 | tf_op jit(solution)/shard_map/all_gather | solution.py:108
  181.0 43.3 %all-reduce.1 = bf16[128,1024]{1,0:T(8,128)(2,1)S(1)} all-reduce(f32[128,1024]{1,0:T(8,128)S(1)} %fusion.30), channel_id=1, replica_groups=mesh['tp'=8,'dp'=4] {'tp'}, use_global_device_ids=true, to_apply=%region_10.11 | all-reduce | flops 131072 | bytes 786432 | tf_op jit(solution)/shard_map/psum | solution.py:111
  228.7 1.9 fusion.24
  230.8 6.0 %psum.23 = f32[128]{0:T(128)S(1)} all-reduce(f32[128]{0:T(128)S(1)} %get-tuple-element.18), channel_id=1, replica_groups=mesh['tp'=8,'dp'=4] {'dp'}, use_global_device_ids=true, to_apply=%region_13.14 | all-reduce | flops 128 | bytes 1024 | tf_op jit(solution)/shard_map/psum | solution.py:76
  243.0 21.7 %reduce-scatter.46.cloned.1.call-done = f32[32,2]{1,0:T(8,128)} async-done(((f32[128,2]{1,0:T(8,128)}), f32[32,2]{1,0:T(8,128)}) %reduce-scatter.46.cloned.1.call-update) | async-done | bytes 272
  266.3 20.5 %reduce-scatter.36.cloned.1.call-done = f32[32,256]{1,0:T(8,128)} async-done(((f32[128,256]{1,0:T(8,128)}), f32[32,256]{1,0:T(8,128)}) %reduce-scatter.36.cloned.1.call-update) | async-done | bytes 32784 | tf_op jit(solution)/shard_map/reduce_scatter | solution.py:69
  286.8 21.9 %reduce-scatter.34.cloned.1.call-done = f32[32,256]{1,0:T(8,128)} async-done(((f32[128,256]{1,0:T(8,128)}), f32[32,256]{1,0:T(8,128)}) %reduce-scatter.34.cloned.1.call-update) | async-done | bytes 32784 | tf_op jit(solution)/shard_map/reduce_scatter | solution.py:70
  308.7 22.7 %reduce-scatter.32.cloned.1.call-done = f32[32,256]{1,0:T(8,128)} async-done(((f32[128,256]{1,0:T(8,128)}), f32[32,256]{1,0:T(8,128)}) %reduce-scatter.32.cloned.1.call-update) | async-done | bytes 32784 | tf_op jit(solution)/shard_map/reduce_scatter | solution.py:71
  332.6 8.6 %fusion.1 = f32[32,2,1,128]{3,2,1,0:T(1,128)S(1)} fusion(f32[32,2,128,1]{2,3,1,0:T(1,128)S(1)} %bitcast.117, f32[2,32,2,128,128]{4,3,2,1,0:T(8,128)} %param.23, f32[32,2,128]{2,1,0:T(2,128)S(1)} %mul.398, f32[32,2,128]{2,1,0:T(2,128)S(1)} %get-tuple-element.23, f32[32,2]{1,0:T(8,128)S(1)} %copy.32), kind=kOutput, calls=%fused_computation.3 | convolution fusion | flops 15728640 | bytes 4325632 | tf_op jit(solution)/shard_map/bhvd,bhd->bhv/dot_general | solution.py:98
  341.5 11.8 %reduce-scatter.30.cloned.1.call-done = f32[32,256]{1,0:T(8,128)} async-done(((f32[128,256]{1,0:T(8,128)}), f32[32,256]{1,0:T(8,128)}) %reduce-scatter.30.cloned.1.call-update) | async-done | bytes 32784 | tf_op jit(solution)/shard_map/reduce_scatter | solution.py:72
  354.1 5.2 %all_gather.11 = bf16[128,256]{1,0:T(8,128)(2,1)S(1)} all-gather(bf16[32,256]{1,0:T(8,128)(2,1)S(1)} %fusion.58), channel_id=1, replica_groups=mesh['tp'=8,'dp'=4] {'dp'}, dimensions={0}, use_global_device_ids=true | all-gather | bytes 81920 | tf_op jit(solution)/shard_map/all_gather | solution.py:108
  361.3 5.4 %multiply_add_fusion.1 = (f32[1,32,2,128,128]{4,3,2,1,0:T(8,128)S(1)}, f32[1,32,2,128,128]{4,3,2,1,0:T(8,128)S(1)}) fusion(f32[2,32,2,128,128]{4,3,2,1,0:T(8,128)} %param.23, f32[32,2,128]{2,1,0:T(2,128)S(1)} %mul.366, f32[32,2,128]{2,1,0:T(2,128)S(1)} %get-tuple-element.25, f32[32,2]{1,0:T(8,128)S(1)} %copy.29, f32[32,2,128]{2,1,0:T(2,128)S(1)} %mul.398, ...), kind=kLoop, calls=%fused_computation.8 | loop fusion | flops 6291456 | bytes 16908800 | tf_op jit(solution)/shard_map/add | solution.py:92
  366.7 4.0 pad_maximum_fusion
  370.7 53.0 %reduce-scatter.38.cloned.1.call-done = f32[16,1024]{1,0:T(8,128)} async-done(((f32[128,1024]{1,0:T(8,128)}), f32[16,1024]{1,0:T(8,128)}) %reduce-scatter.38.cloned.1.call-update) | async-done | bytes 65552 | tf_op jit(solution)/shard_map/reduce_scatter | solution.py:17
  (99 shorter events, 32.6 us)
Async XLA Ops:
  7.2 43.0 %copy-start.1 = (bf16[2,1024,256]{2,1,0:T(8,128)(2,1)S(1)}, bf16[2,1024,256]{2,1,0:T(8,128)(2,1)}, u32[]{:S(2)}) copy-start(bf16[2,1024,256]{2,1,0:T(8,128)(2,1)} %param.14) | copy-start | bytes 3145732
  7.2 44.0 %copy-start.2 = (bf16[2,1024,256]{2,1,0:T(8,128)(2,1)S(1)}, bf16[2,1024,256]{2,1,0:T(8,128)(2,1)}, u32[]{:S(2)}) copy-start(bf16[2,1024,256]{2,1,0:T(8,128)(2,1)} %param.17) | copy-start | bytes 3145732
  7.2 45.1 %copy-start.4 = (f32[2,256]{1,0:T(2,128)S(1)}, f32[2,256]{1,0:T(2,128)}, u32[]{:S(2)}) copy-start(f32[2,256]{1,0:T(2,128)} %param.21) | copy-start | bytes 6148
  7.2 79.8 %copy-start.5 = (f32[2,32,2]{1,2,0:T(2,128)S(1)}, f32[2,32,2]{1,2,0:T(2,128)}, u32[]{:S(2)}) copy-start(f32[2,32,2]{1,2,0:T(2,128)} %param.25) | copy-start | bytes 1540
  7.2 146.5 %copy-start.3 = (f32[2,32,2,128]{3,2,1,0:T(2,128)S(1)}, f32[2,32,2,128]{3,2,1,0:T(2,128)}, u32[]{:S(2)}) copy-start(f32[2,32,2,128]{3,2,1,0:T(2,128)} %param.24) | copy-start | bytes 196612
  7.2 57.0 %reduce-scatter.42.cloned.1.call-start = ((), (), s32[]{:S(2)}) async-start(), calls=%async_computation.23 | async-start | bytes 81920
  43.5 42.7 %reduce-scatter.40.cloned.1.call-start = ((), (), s32[]{:S(2)}) async-start(), calls=%async_computation.22 | async-start | bytes 81920
  46.1 62.8 %reduce-scatter.24.cloned.1.call-start = ((), (), s32[]{:S(2)}) async-start(), calls=%async_computation.14 | async-start | bytes 163840 | tf_op jit(solution)/shard_map/reduce_scatter | solution.py:71
  48.1 82.7 %reduce-scatter.26.cloned.1.call-start = ((), (), s32[]{:S(2)}) async-start(), calls=%async_computation.15 | async-start | bytes 163840 | tf_op jit(solution)/shard_map/reduce_scatter | solution.py:70
  50.1 102.6 %reduce-scatter.28.cloned.1.call-start = ((), (), s32[]{:S(2)}) async-start(), calls=%async_computation.16 | async-start | bytes 163840 | tf_op jit(solution)/shard_map/reduce_scatter | solution.py:69
  51.0 129.7 %copy-start = (bf16[2,256,1024]{2,1,0:T(8,128)(2,1)S(1)}, bf16[2,256,1024]{2,1,0:T(8,128)(2,1)}, u32[]{:S(2)}) copy-start(bf16[2,256,1024]{2,1,0:T(8,128)(2,1)} %param.22) | copy-start | bytes 3145732
  51.1 123.6 %reduce-scatter.22.cloned.1.call-start = ((), (), s32[]{:S(2)}) async-start(), calls=%async_computation.13 | async-start | bytes 163840 | tf_op jit(solution)/shard_map/reduce_scatter | solution.py:72
  52.1 190.1 %reduce-scatter.44.cloned.1.call-start = ((), (), s32[]{:S(2)}) async-start(), calls=%async_computation.24 | async-start | bytes 81920
  226.0 38.6 %reduce-scatter.46.cloned.1.call-start = ((), (), s32[]{:S(2)}) async-start(), calls=%async_computation.25 | async-start | bytes 81920
  227.7 59.0 %reduce-scatter.36.cloned.1.call-start = ((), (), s32[]{:S(2)}) async-start(), calls=%async_computation.20 | async-start | bytes 163840 | tf_op jit(solution)/shard_map/reduce_scatter | solution.py:69
  228.7 80.0 %reduce-scatter.34.cloned.1.call-start = ((), (), s32[]{:S(2)}) async-start(), calls=%async_computation.19 | async-start | bytes 163840 | tf_op jit(solution)/shard_map/reduce_scatter | solution.py:70
  230.7 100.7 %reduce-scatter.32.cloned.1.call-start = ((), (), s32[]{:S(2)}) async-start(), calls=%async_computation.18 | async-start | bytes 163840 | tf_op jit(solution)/shard_map/reduce_scatter | solution.py:71
  238.7 114.6 %reduce-scatter.30.cloned.1.call-start = ((), (), s32[]{:S(2)}) async-start(), calls=%async_computation.17 | async-start | bytes 163840 | tf_op jit(solution)/shard_map/reduce_scatter | solution.py:72
  240.8 182.8 %reduce-scatter.38.cloned.1.call-start = ((), (), s32[]{:S(2)}) async-start(), calls=%async_computation.21 | async-start | bytes 589824 | tf_op jit(solution)/shard_map/reduce_scatter | solution.py:17
Sparse Core Ops, SparseCore 0:
  43.6 20.5 reduce-scatter.41
  66.6 19.5 reduce-scatter.39
  89.2 19.6 reduce-scatter.23
  111.1 19.6 reduce-scatter.25
  133.1 19.6 reduce-scatter.27
  155.0 19.6 reduce-scatter.21
  226.2 15.9 reduce-scatter.43
  245.1 19.4 reduce-scatter.45
  267.1 19.6 reduce-scatter.35
  289.1 19.6 reduce-scatter.33
  311.7 19.6 reduce-scatter.31
  333.6 19.6 reduce-scatter.29
  360.6 63.0 reduce-scatter.37
where the time goes:
time: 433 us; the launch traced here: 432 us
  waiting for transfers between devices  258 us (60%)
  blocking collectives  98.2 us (23%)
  matrix products  35.8 us (8%)
  other arithmetic  17.3 us (4%)
  between operations  14.2 us (3%)
  local copies, waits for them, and re-layouts  7.86 us (2%)
    reduce_scatter x1, waiting for transfers between devices, spread_heads(): return lax.psum_scatter(out_part, 'tp', scatter_dimension=0, tiled=True)  53 us
    unnamed x17, waiting for transfers between devices  50.6 us
    reduce_scatter x2, waiting for transfers between devices, per_device(): lax.psum_scatter(value_part, 'dp', scatter_dimension=0, tiled=True)  44.3 us
    reduce_scatter x2, waiting for transfers between devices, per_device(): lax.psum_scatter(key_part, 'dp', scatter_dimension=0, tiled=True)  43.9 us
    psum x1, blocking collectives, per_device(): gathered = lax.psum(out_part, 'tp').astype(jnp.bfloat16)  43.3 us
    reduce_scatter x2, waiting for transfers between devices, per_device(): lax.psum_scatter(query_part, 'dp', scatter_dimension=0, tiled=True)  42.4 us
    all_gather x1, blocking collectives, gather_rows(): return lax.all_gather(block_input, 'tp', axis=0, tiled=True)  32.8 us
    reduce_scatter x2, waiting for transfers between devices, per_device(): lax.psum_scatter(outgate_part, 'dp', scatter_dimension=0, tiled=True)  23.6 us
  transfers between devices with their start and end apart: 13, of which 13 were waited for; matrix products, arithmetic and copies ran while one was open for 12% of the time, Pallas kernels for 0%

commit v1 on v0

v1 whole, which is shorter than its diff:
```python
import functools
import math

import jax
import jax.numpy as jnp
from jax import lax
from jax.experimental import pallas as pl
from jax.experimental.pallas import tpu as pltpu
from jax.sharding import PartitionSpec as P

EPSILON = 1e-06
F32 = jnp.float32
BF16 = jnp.bfloat16
MESH = pl.DeviceIdType.MESH


def split_axis(size):
    inner = max(f for f in range(1, math.isqrt(size) + 1) if size % f == 0)
    return size // inner, inner


def row_block(index, rows):
    return pl.ds(pl.multiple_of(index * rows, rows), rows)


def gate_dot(scaled, weight):
    return lax.dot_general(
        scaled, weight, (((1,), (1,)), ((), ())), preferred_element_type=F32
    )


def step_kernel(
    ntp,
    ndp,
    tokens,
    wq,
    wk,
    wv,
    wo,
    wig,
    wfg,
    norm_gain,
    head_gain,
    proj,
    cell,
    normer,
    stab,
    final_out,
    value_out,
    key_out,
    normer_out,
    aux_out,
    stab_out,
    w_buf,
    ig_buf,
    fg_buf,
    proj_buf,
    cell_buf,
    tok_sem,
    small_sem,
    gain_buf,
    head_buf,
    normer_buf,
    stab_buf,
    split_buf,
    current,
    partial,
    gates,
    pair_recv,
    pair_gate,
    pair_sum,
    pair_gsum,
    proj_recv,
    gate_recv,
    query_buf,
    read_buf,
    gated_all,
    out_part,
    out_stage,
    out_recv,
    load_sem,
    cell_sem,
    ag_send,
    ag_recv,
    pr_send,
    pr_recv,
    pg_send,
    pg_recv,
    rs_send,
    rs_recv,
    gt_send,
    gt_recv,
    gg_send,
    gg_recv,
    os_send,
    os_recv,
):
    blocks = wq.shape[0]
    width, inner = wq.shape[1], wq.shape[2]
    all_heads = wig.shape[1]
    seqs, heads, dh = cell.shape[1], cell.shape[2], cell.shape[3]
    rows = tokens.shape[0]
    t = lax.axis_index("tp")
    d = lax.axis_index("dp")
    outer, side = split_axis(ntp)
    z = t // side
    x = lax.rem(t, side)

    pair = 2 if ndp % 2 == 0 else 1
    ring = ndp // pair
    y = d // pair
    core = lax.rem(d, pair)

    tok_load = pltpu.make_async_copy(tokens, current.at[0, row_block(t, rows)], tok_sem)
    tok_load.start()
    small = [
        pltpu.make_async_copy(src, dst, small_sem.at[i])
        for i, (src, dst) in enumerate(
            (
                (norm_gain, gain_buf),
                (head_gain, head_buf),
                (normer, normer_buf),
                (stab, stab_buf),
            )
        )
    ]
    loads = []
    for b in range(blocks):
        for i, w in enumerate((wq, wk, wv, wo)):
            loads.append(pltpu.make_async_copy(w.at[b], w_buf.at[b, i], load_sem.at[b, i]))
        loads.append(
            pltpu.make_async_copy(
                wig.at[b, :, row_block(d, width)], ig_buf.at[b], load_sem.at[b, 4]
            )
        )
        loads.append(
            pltpu.make_async_copy(
                wfg.at[b, :, row_block(d, width)], fg_buf.at[b], load_sem.at[b, 5]
            )
        )
        loads.append(pltpu.make_async_copy(proj.at[b], proj_buf.at[b], load_sem.at[b, 6]))
    cell_loads = [
        pltpu.make_async_copy(cell.at[b], cell_buf.at[b], cell_sem.at[b]) for b in range(blocks)
    ]
    per_block = 7
    for b in range(blocks):
        for c in loads[b * per_block : (b + 1) * per_block]:
            c.start()
        cell_loads[b].start()
        if b == 0:
            for c in small:
                c.start()

    barrier = pltpu.get_barrier_semaphore()
    for k in range(1, ntp):
        pl.semaphore_signal(
            barrier, inc=1, device_id={"tp": lax.rem(t + k, ntp)}, device_id_type=MESH
        )
    for k in range(1, ndp):
        pl.semaphore_signal(
            barrier, inc=1, device_id={"dp": lax.rem(d + k, ndp)}, device_id_type=MESH
        )
    pl.semaphore_wait(barrier, ntp - 1 + ndp - 1)
    tok_load.wait()

    def split_cells(b):
        cell_loads[b].wait()

        def one(i, _):
            for h in range(heads):
                whole = cell_buf[b, i, h]
                high = whole.astype(BF16)
                split_buf[i, h, :, 0:dh] = high
                split_buf[i, h, :, dh : 2 * dh] = (whole - high.astype(F32)).astype(BF16)
            return 0

        lax.fori_loop(0, seqs, one, 0)

    def gather(b):
        buf = current.at[b]
        own_src = buf.at[row_block(t, rows)]

        def send(src, block, slot, dest):
            copy = pltpu.make_async_remote_copy(
                src_ref=src,
                dst_ref=buf.at[row_block(block, rows)],
                send_sem=ag_send.at[b, slot],
                recv_sem=ag_recv.at[b, slot],
                device_id={"tp": dest},
                device_id_type=MESH,
            )
            copy.start()
            return copy

        first, second = [], []
        for k in range(1, outer):
            dest = lax.rem(z + k, outer) * side + x
            first.append(send(own_src, t, k - 1, dest))
        for j in range(1, side):
            dest = z * side + lax.rem(x + j, side)
            second.append(send(own_src, t, outer - 1 + (j - 1) * outer, dest))
        if b == 0:
            split_cells(0)
            for c in small:
                c.wait()
        for k in range(1, outer):
            first[k - 1].wait_recv()
            block = lax.rem(z - k + outer, outer) * side + x
            for j in range(1, side):
                dest = z * side + lax.rem(x + j, side)
                second.append(
                    send(
                        buf.at[row_block(block, rows)],
                        block,
                        outer - 1 + (j - 1) * outer + k,
                        dest,
                    )
                )
        for c in second:
            c.wait_recv()
        for c in first + second:
            c.wait_send()

    for b in range(blocks):
        gather(b)
        for c in loads[b * per_block : (b + 1) * per_block]:
            c.wait()
        as_float = current[b].astype(F32)
        scaled = (as_float * gain_buf[b : b + 1, :]).astype(BF16)
        gates[b, :, 0:all_heads] = gate_dot(scaled, ig_buf[b])
        gates[b, :, all_heads : 2 * all_heads] = gate_dot(scaled, fg_buf[b])
        gates[b, :, 2 * all_heads : 2 * all_heads + 1] = jnp.sum(
            as_float * as_float, axis=1, keepdims=True
        )
        sends = []

        def send_rows(srcs, dsts, send_sems, recv_sems, slot, dest):
            started = []
            for src, dst, ss, rr in zip(srcs, dsts, send_sems, recv_sems):
                copy = pltpu.make_async_remote_copy(
                    src_ref=src,
                    dst_ref=dst,
                    send_sem=ss.at[b, slot],
                    recv_sem=rr.at[b, slot],
                    device_id={"dp": dest},
                    device_id_type=MESH,
                )
                copy.start()
                started.append(copy)
            sends.extend(started)
            return started

        for i in range(4):
            cols = slice(i * inner, (i + 1) * inner)
            partial[b, :, cols] = jnp.dot(scaled, w_buf[b, i], preferred_element_type=F32)
        paired = []
        if pair == 2:
            mate = y * pair + 1 - core
            for k in range(ring):
                slot = (k + 1) % ring
                block = row_block(lax.rem(y + slot, ring) * pair + 1 - core, seqs)
                paired.append(
                    (
                        slot,
                        send_rows(
                            (partial.at[b, block], gates.at[b, block]),
                            (pair_recv.at[b, slot], pair_gate.at[b, slot]),
                            (pr_send, pg_send),
                            (pr_recv, pg_recv),
                            slot,
                            mate,
                        ),
                    )
                )
        else:
            paired = [((k + 1) % ring, []) for k in range(ring)]
        arriving = []
        total = gate_sum = None
        for slot, copies in paired:
            for c in copies:
                c.wait_recv()
            dest = lax.rem(y + slot, ring) * pair + core
            block = row_block(dest, seqs)
            rows_sum, gsum = partial[b, block, :], gates[b, block, :]
            if copies:
                rows_sum = rows_sum + pair_recv[b, slot]
                gsum = gsum + pair_gate[b, slot]
            if slot == 0:
                total, gate_sum = rows_sum, gsum
            else:
                pair_sum[b, slot - 1] = rows_sum.astype(pair_sum.dtype)
                pair_gsum[b, slot - 1] = gsum
                arriving.append(
                    send_rows(
                        (pair_sum.at[b, slot - 1], pair_gsum.at[b, slot - 1]),
                        (proj_recv.at[b, slot - 1], gate_recv.at[b, slot - 1]),
                        (rs_send, gt_send),
                        (rs_recv, gt_recv),
                        slot - 1,
                        dest,
                    )
                )
        for k in range(ring - 1):
            for c in arriving[k]:
                c.wait_recv()
            total = total + proj_recv[b, k].astype(F32)
            gate_sum = gate_sum + gate_recv[b, k]
        own = row_block(d, seqs)
        inv_rms = lax.rsqrt(gate_sum[:, 2 * all_heads : 2 * all_heads + 1] / (width * ndp) + EPSILON)
        query = total[:, 0:inner] * inv_rms
        key = total[:, inner : 2 * inner] * inv_rms * (dh ** (-0.5))
        value = total[:, 2 * inner : 3 * inner] * inv_rms
        outgate = total[:, 3 * inner : 4 * inner] * inv_rms
        pre = gate_sum * inv_rms
        query_buf[...] = query
        key_out[b] = key
        def read_chunk(c, _):
            eight = pl.ds(pl.multiple_of(c * 8, 8), 8)
            sub = lax.broadcasted_iota(jnp.int32, (8, dh), 0)
            for h in range(heads):
                lanes = slice(h * dh, (h + 1) * dh)
                q8 = query_buf[eight, lanes]
                high = q8.astype(BF16)
                low = (q8 - high.astype(F32)).astype(BF16)
                high, low = jnp.concatenate([high, high], 1), jnp.concatenate([low, low], 1)
                lhs = jnp.concatenate([high, low], 0)
                acc = jnp.zeros((8, dh), F32)
                for j in range(8):
                    prod = lax.dot_general(
                        lhs,
                        split_buf[c * 8 + j, h],
                        (((1,), (1,)), ((), ())),
                        preferred_element_type=F32,
                    )
                    acc = jnp.where(sub == j, prod[0:8] + prod[8:16], acc)
                read_buf[eight, lanes] = acc
            return 0

        lax.fori_loop(0, seqs // 8, read_chunk, 0)

        lane = lax.broadcasted_iota(jnp.int32, pre.shape, 1)
        aux = jnp.zeros(pre.shape, F32)
        for h in range(heads):
            lanes = slice(h * dh, (h + 1) * dh)
            head = t * heads + h
            igate = jnp.sum(jnp.where(lane == head, pre, 0.0), axis=1, keepdims=True)
            fpre = jnp.sum(jnp.where(lane == head + all_heads, pre, 0.0), axis=1, keepdims=True)
            lf = jnp.minimum(fpre, 0.0) - jnp.log1p(jnp.exp(-jnp.abs(fpre)))
            stab_row = jnp.broadcast_to(stab_buf[b, h : h + 1, :], (seqs, seqs))
            diag = lax.broadcasted_iota(jnp.int32, (seqs, seqs), 0) == (
                lax.broadcasted_iota(jnp.int32, (seqs, seqs), 1)
            )
            m0 = jnp.sum(jnp.where(diag, stab_row, 0.0), axis=1, keepdims=True)
            carried = lf + m0
            m1 = jnp.maximum(carried, igate)
            stab_out[b, h : h + 1, :] = jnp.sum(jnp.where(diag, m1, 0.0), axis=0, keepdims=True)
            keep = jnp.exp(carried - m1)
            write = jnp.exp(igate - m1)
            qh, kh = query[:, lanes], key[:, lanes]
            written = write * value[:, lanes]
            n1 = keep * normer_buf[b, :, h, :] + write * kh
            value_out[b, :, lanes] = written
            normer_out[b, :, lanes] = n1
            aux = jnp.where(lane == h, keep, aux)
            numer = keep * read_buf[:, lanes] + written * jnp.sum(kh * qh, axis=1, keepdims=True)
            denom = jnp.maximum(jnp.abs(jnp.sum(n1 * qh, axis=1, keepdims=True)), 1.0)
            readout = numer / denom
            normed = readout * lax.rsqrt(
                jnp.mean(readout * readout, axis=1, keepdims=True) + EPSILON
            )
            normed = normed * head_buf[b : b + 1, lanes]
            gate = 1.0 / (1.0 + jnp.exp(-outgate[:, lanes]))
            gated_all[b, own, lanes] = (gate * normed).astype(BF16)
        aux_out[b] = aux

        spread = []
        for k in range(1, ndp):
            copy = pltpu.make_async_remote_copy(
                src_ref=gated_all.at[b, own],
                dst_ref=gated_all.at[b, own],
                send_sem=gg_send.at[b, k - 1],
                recv_sem=gg_recv.at[b, k - 1],
                device_id={"dp": lax.rem(d + k, ndp)},
                device_id_type=MESH,
            )
            copy.start()
            spread.append(copy)
        for c in spread:
            c.wait_recv()
        part = jnp.dot(gated_all[b], proj_buf[b], preferred_element_type=F32)
        out_part[...] = part
        out_stage[b] = part.astype(BF16)
        outs = []
        for k in range(1, ntp):
            dest = lax.rem(t + k, ntp)
            copy = pltpu.make_async_remote_copy(
                src_ref=out_stage.at[b, row_block(dest, rows)],
                dst_ref=out_recv.at[b, k - 1],
                send_sem=os_send.at[b, k - 1],
                recv_sem=os_recv.at[b, k - 1],
                device_id={"tp": dest},
                device_id_type=MESH,
            )
            copy.start()
            outs.append(copy)
        if b + 1 < blocks:
            split_cells(b + 1)
        for c in outs:
            c.wait_recv()
        summed = out_part[row_block(t, rows), :]
        for k in range(ntp - 1):
            summed = summed + out_recv[b, k].astype(F32)
        if b + 1 < blocks:
            current[b + 1, row_block(t, rows), :] = summed.astype(BF16)
        else:
            final_out[...] = summed.astype(BF16)
        for c in sends + spread + outs:
            c.wait_send()


def update_kernel(
    cell, value, key, aux, normer, stab_in, rows_in, cell_out, normer_out, stab_out, rows_out
):
    chunk, heads, dh = cell.shape[1], cell.shape[2], cell.shape[3]
    b = pl.program_id(0)
    here = row_block(pl.program_id(1), chunk)
    keep = aux[b, here, :]
    for h in range(heads):
        lanes = slice(h * dh, (h + 1) * dh)
        across = jnp.transpose(value[b, here, lanes])
        keys = key[b, here, lanes]
        for j in range(chunk):
            cell_out[0, j, h] = (
                keep[j : j + 1, h : h + 1] * cell[0, j, h]
                + across[:, j : j + 1] * keys[j : j + 1, :]
            )
        normer_out[0, :, h, :] = normer[b, here, lanes]
    stab_out[...] = stab_in[...]
    rows_out[...] = rows_in[...]


def origin(ndim, b, c):
    return (0,) * ndim


def per_device(ntp, ndp, *args):
    (tokens, wq, wk, wv, wo, wig, wfg, norm_gain, head_gain, proj, cell, normer, stab) = args
    blocks, width, inner = wq.shape
    all_heads = wig.shape[2]
    seqs, heads, dh = cell.shape[1], cell.shape[2], cell.shape[3]
    rows = tokens.shape[0]
    pair = 2 if ndp % 2 == 0 else 1
    ring = ndp // pair
    more = max(ring - 1, 1)
    wig, wfg, stab = (jnp.swapaxes(a, 1, 2) for a in (wig, wfg, stab))
    batch = rows * ntp
    lanes = -(-(2 * all_heads + 1) // 128) * 128
    hbm = pl.BlockSpec(memory_space=pltpu.HBM)
    dma = pltpu.SemaphoreType.DMA
    final_rows, value, key, normer_rows, aux, stab_rows = pl.pallas_call(
        functools.partial(step_kernel, ntp, ndp),
        out_shape=(
            jax.ShapeDtypeStruct(tokens.shape, BF16),
            jax.ShapeDtypeStruct((blocks, seqs, inner), F32),
            jax.ShapeDtypeStruct((blocks, seqs, inner), F32),
            jax.ShapeDtypeStruct((blocks, seqs, inner), F32),
            jax.ShapeDtypeStruct((blocks, seqs, lanes), F32),
            jax.ShapeDtypeStruct(stab.shape, F32),
        ),
        in_specs=[hbm] * 13,
        out_specs=(pl.BlockSpec(),) * 6,
        scratch_shapes=[
            pltpu.VMEM((blocks, 4, width, inner), BF16),
            pltpu.VMEM((blocks, all_heads, width), BF16),
            pltpu.VMEM((blocks, all_heads, width), BF16),
            pltpu.VMEM(proj.shape, BF16),
            pltpu.VMEM(cell.shape, F32),
            dma,
            dma((4,)),
            pltpu.VMEM(norm_gain.shape, F32),
            pltpu.VMEM(head_gain.shape, F32),
            pltpu.VMEM(normer.shape, F32),
            pltpu.VMEM(stab.shape, F32),
            pltpu.VMEM((seqs, heads, dh, 2 * dh), BF16),
            pltpu.VMEM((blocks, batch, width), BF16),
            pltpu.VMEM((blocks, batch, 4 * inner), F32),
            pltpu.VMEM((blocks, batch, lanes), F32),
            pltpu.VMEM((blocks, ring, seqs, 4 * inner), F32),
            pltpu.VMEM((blocks, ring, seqs, lanes), F32),
            pltpu.VMEM((blocks, more, seqs, 4 * inner), F32),
            pltpu.VMEM((blocks, more, seqs, lanes), F32),
            pltpu.VMEM((blocks, more, seqs, 4 * inner), F32),
            pltpu.VMEM((blocks, more, seqs, lanes), F32),
            pltpu.VMEM((seqs, inner), F32),
            pltpu.VMEM((seqs, inner), F32),
            pltpu.VMEM((blocks, batch, inner), BF16),
            pltpu.VMEM((batch, width), F32),
            pltpu.VMEM((blocks, batch, width), BF16),
            pltpu.VMEM((blocks, ntp - 1, rows, width), BF16),
            dma((blocks, 7)),
            dma((blocks,)),
            dma((blocks, ntp - 1)),
            dma((blocks, ntp - 1)),
            dma((blocks, ring)),
            dma((blocks, ring)),
            dma((blocks, ring)),
            dma((blocks, ring)),
            dma((blocks, more)),
            dma((blocks, more)),
            dma((blocks, more)),
            dma((blocks, more)),
            dma((blocks, ndp - 1)),
            dma((blocks, ndp - 1)),
            dma((blocks, ntp - 1)),
            dma((blocks, ntp - 1)),
        ],
        compiler_params=pltpu.CompilerParams(
            collective_id=0, has_side_effects=True, vmem_limit_bytes=67_043_328
        ),
    )(tokens, wq, wk, wv, wo, wig, wfg, norm_gain, head_gain, proj, cell, normer, stab)

    chunk = math.gcd(seqs, 8)
    whole_rows = pl.BlockSpec(tokens.shape, lambda b, c: (0, 0))
    whole_stab = pl.BlockSpec(stab.shape, lambda b, c: (0, 0, 0))
    cell_spec = pl.BlockSpec((1, chunk, heads, dh, dh), lambda b, c: (b, c, 0, 0, 0))
    cell_out, normer_out, stab_out, rows_out = pl.pallas_call(
        update_kernel,
        grid=(blocks, seqs // chunk),
        out_shape=(
            jax.ShapeDtypeStruct(cell.shape, F32),
            jax.ShapeDtypeStruct(normer.shape, F32),
            jax.ShapeDtypeStruct(stab.shape, F32),
            jax.ShapeDtypeStruct(tokens.shape, BF16),
        ),
        in_specs=[cell_spec]
        + [
            pl.BlockSpec(a.shape, functools.partial(origin, a.ndim))
            for a in (value, key, aux, normer_rows, stab_rows, final_rows)
        ],
        out_specs=(
            cell_spec,
            pl.BlockSpec((1, chunk, heads, dh), lambda b, c: (b, c, 0, 0)),
            whole_stab,
            whole_rows,
        ),
    )(cell, value, key, aux, normer_rows, stab_rows, final_rows)
    return rows_out, cell_out, normer_out, jnp.swapaxes(stab_out, 1, 2)


def solution(mesh):
    return jax.shard_map(
        functools.partial(per_device, mesh.shape["tp"], mesh.shape["dp"]),
        mesh=mesh,
        in_specs=(
            P("tp", "dp"),
            P(None, "dp", "tp"),
            P(None, "dp", "tp"),
            P(None, "dp", "tp"),
            P(None, "dp", "tp"),
            P(),
            P(),
            P(None, "dp"),
            P(None, "tp"),
            P(None, "tp", "dp"),
            P(None, "dp", "tp", None, None),
            P(None, "dp", "tp", None),
            P(None, "dp", "tp"),
        ),
        out_specs=(
            P("tp", "dp"),
            P(None, "dp", "tp", None, None),
            P(None, "dp", "tp", None),
            P(None, "dp", "tp"),
        ),
        check_vma=False,
    )
```

time: 433 us -> 71 us (0.16)
  waiting for transfers between devices: 258 us -> 0 us
  blocking collectives: 98.2 us -> 0 us
  Pallas kernels: 0 us -> 70.1 us
  matrix products: 35.8 us -> 0 us
  other arithmetic: 17.3 us -> 0 us
  between operations: 14.2 us -> 0.64 us
  local copies, waits for them, and re-layouts: 7.86 us -> 0 us
    reduce_scatter x9 -> x0, waiting for transfers between devices: 207 us -> none  [the longest x1 53 us: spread_heads(): return lax.psum_scatter(out_part, 'tp', scatter_dimension=0, tiled=True)]
    pallas_call x0 -> x2, Pallas kernels: none -> 70.1 us  [the longest x1 59.4 us: per_device(): pl.pallas_call(functools.partial(step_kernel, ntp, ndp), out_shape=(jax.S...]
    psum x3 -> x0, blocking collectives: 54.9 us -> none  [the longest x1 43.3 us: per_device(): gathered = lax.psum(out_part, 'tp').astype(jnp.bfloat16)]
    unnamed x17 -> x0, waiting for transfers between devices: 50.6 us -> none
    all_gather x3 -> x0, blocking collectives: 43.2 us -> none  [the longest x1 32.8 us: gather_rows(): return lax.all_gather(block_input, 'tp', axis=0, tiled=True)]
    dot_general x12 -> x0, matrix products: 30.8 us -> none  [the longest x2 17.2 us: per_device(): jnp.einsum('bhvd,bhd->bhv', new_cell, query_rows, precision=lax.Precision...]
    add x2 -> x0, other arithmetic: 5.58 us -> none  [the longest x1 5.38 us: per_device(): keep_rate[..., None, None] * cell_state[layer_num]]
    another operation x5 -> x0, other arithmetic: 5.27 us -> none  [the longest x1 3.98 us: per_device(): jnp.stack(cell_list)]
  transfers between devices with their start and end apart: 13 -> 0, of which waited for: 13 -> 0; matrix products, arithmetic and copies ran while one was open for 12% -> 0% of each run, Pallas kernels for 0% -> 0%
where the time goes in v1:
time: 71 us; the launch traced here: 70.7 us
  Pallas kernels  70.1 us (99%)
    pallas_call x1, Pallas kernels, per_device(): pl.pallas_call(functools.partial(step_kernel, ntp, ndp), out_shape=(jax.S...  59.4 us
    pallas_call x1, Pallas kernels, per_device(): pl.pallas_call(update_kernel, grid=(blocks, seqs // chunk), out_shape=(ja...  10.7 us

profile of v1, /device:TPU:0, one launch (start us, length us, event | category | flops | bytes accessed | tf_op | source)
XLA Modules:
  0.0 70.7 jit_solution(4693029931400294122)
XLA Ops:
  0.6 59.4 %shard_map.156 = (bf16[16,1024]{1,0:T(8,128)(2,1)}, f32[2,32,256]{2,1,0:T(8,128)}, f32[2,32,256]{2,1,0:T(8,128)}, f32[2,32,256]{2,1,0:T(8,128)}, f32[2,32,128]{2,1,0:T(8,128)}, /*index=5*/f32[2,2,32]{2,1,0:T(2,128)}) custom-call(bf16[16,1024]{1,0:T(8,128)(2,1)} %tokens.1, bf16[2,1024,256]{2,1,0:T(8,128)(2,1)} %wq.1, bf16[2,1024,256]{2,1,0:T(8,128)(2,1)} %wk.1, ...), custom_call_target="tpu_custom_call" | custom-call | tf_op jit(solution)/shard_map/pallas_call | solution.py:460
  60.0 10.7 %shard_map.157 = (f32[2,32,2,128,128]{4,3,2,1,0:T(8,128)}, f32[2,32,2,128]{3,2,1,0:T(2,128)}, f32[2,2,32]{2,1,0:T(2,128)}, bf16[16,1024]{1,0:T(8,128)(2,1)}) custom-call(f32[2,32,2,128,128]{4,3,2,1,0:T(8,128)} %cell.3, f32[2,32,256]{2,1,0:T(8,128)} %get-tuple-element.14.value, f32[2,32,256]{2,1,0:T(8,128)} %get-tuple-element.15.key, ...), custom_call_target="tpu_custom_call" | custom-call | tf_op jit(solution)/shard_map/pallas_call | solution.py:526

commit v2 on v1

--- a/solution.py
+++ b/solution.py
@@ -46,16 +46,16 @@
     normer,
     stab,
     final_out,
-    value_out,
-    key_out,
+    cell_buf,
     normer_out,
-    aux_out,
     stab_out,
     w_buf,
     ig_buf,
     fg_buf,
     proj_buf,
-    cell_buf,
+    written_buf,
+    key_buf,
+    keep_buf,
     tok_sem,
     small_sem,
     gain_buf,
@@ -72,8 +72,6 @@
     pair_gsum,
     proj_recv,
     gate_recv,
-    query_buf,
-    read_buf,
     gated_all,
     out_part,
     out_stage,
@@ -170,11 +168,31 @@
             for h in range(heads):
                 whole = cell_buf[b, i, h]
                 high = whole.astype(BF16)
-                split_buf[i, h, :, 0:dh] = high
-                split_buf[i, h, :, dh : 2 * dh] = (whole - high.astype(F32)).astype(BF16)
+                here = row_block(i, dh)
+                split_buf[h, here, 0:dh] = high
+                split_buf[h, here, dh : 2 * dh] = (whole - high.astype(F32)).astype(BF16)
             return 0
 
         lax.fori_loop(0, seqs, one, 0)
+
+    eight = math.gcd(seqs, 8)
+
+    def update_cells(b):
+        def one(c, _):
+            here = row_block(c, eight)
+            keep = keep_buf[here, :]
+            for h in range(heads):
+                lanes = slice(h * dh, (h + 1) * dh)
+                across = jnp.transpose(written_buf[here, lanes])
+                keys = key_buf[here, lanes]
+                for j in range(eight):
+                    cell_buf[b, c * eight + j, h] = (
+                        keep[j : j + 1, h : h + 1] * cell_buf[b, c * eight + j, h]
+                        + across[:, j : j + 1] * keys[j : j + 1, :]
+                    )
+            return 0
+
+        lax.fori_loop(0, seqs // eight, one, 0)
 
     def gather(b):
         buf = current.at[b]
@@ -312,31 +330,28 @@
         value = total[:, 2 * inner : 3 * inner] * inv_rms
         outgate = total[:, 3 * inner : 4 * inner] * inv_rms
         pre = gate_sum * inv_rms
-        query_buf[...] = query
-        key_out[b] = key
-        def read_chunk(c, _):
-            eight = pl.ds(pl.multiple_of(c * 8, 8), 8)
-            sub = lax.broadcasted_iota(jnp.int32, (8, dh), 0)
-            for h in range(heads):
-                lanes = slice(h * dh, (h + 1) * dh)
-                q8 = query_buf[eight, lanes]
-                high = q8.astype(BF16)
-                low = (q8 - high.astype(F32)).astype(BF16)
-                high, low = jnp.concatenate([high, high], 1), jnp.concatenate([low, low], 1)
-                lhs = jnp.concatenate([high, low], 0)
-                acc = jnp.zeros((8, dh), F32)
-                for j in range(8):
-                    prod = lax.dot_general(
-                        lhs,
-                        split_buf[c * 8 + j, h],
-                        (((1,), (1,)), ((), ())),
-                        preferred_element_type=F32,
-                    )
-                    acc = jnp.where(sub == j, prod[0:8] + prod[8:16], acc)
-                read_buf[eight, lanes] = acc
-            return 0
-
-        lax.fori_loop(0, seqs // 8, read_chunk, 0)
+        key_buf[...] = key
+        wide = -(-2 * seqs // 128) * 128
+        column = lax.broadcasted_iota(jnp.int32, (dh, wide), 1)
+        reads = []
+        for h in range(heads):
+            lanes = slice(h * dh, (h + 1) * dh)
+            high = query[:, lanes].astype(BF16)
+            low = (query[:, lanes] - high.astype(F32)).astype(BF16)
+            terms = [jnp.concatenate([a, a], 1) for a in (high, low)]
+            if wide > 2 * seqs:
+                terms.append(jnp.zeros((wide - 2 * seqs, 2 * dh), BF16))
+            rhs = jnp.concatenate(terms, 0)
+            acc = jnp.zeros((dh, wide), F32)
+            for c in range(seqs // eight):
+                prod = gate_dot(
+                    split_buf[h, c * eight * dh : (c + 1) * eight * dh, :], rhs
+                )
+                for j in range(eight):
+                    own_column = (column == c * eight + j) | (column == seqs + c * eight + j)
+                    acc = jnp.where(own_column, prod[j * dh : (j + 1) * dh], acc)
+            turned = jnp.transpose(acc)
+            reads.append(turned[0:seqs] + turned[seqs : 2 * seqs])
 
         lane = lax.broadcasted_iota(jnp.int32, pre.shape, 1)
         aux = jnp.zeros(pre.shape, F32)
@@ -359,10 +374,10 @@
             qh, kh = query[:, lanes], key[:, lanes]
             written = write * value[:, lanes]
             n1 = keep * normer_buf[b, :, h, :] + write * kh
-            value_out[b, :, lanes] = written
-            normer_out[b, :, lanes] = n1
+            written_buf[:, lanes] = written
+            normer_out[b, :, h, :] = n1
             aux = jnp.where(lane == h, keep, aux)
-            numer = keep * read_buf[:, lanes] + written * jnp.sum(kh * qh, axis=1, keepdims=True)
+            numer = keep * reads[h] + written * jnp.sum(kh * qh, axis=1, keepdims=True)
             denom = jnp.maximum(jnp.abs(jnp.sum(n1 * qh, axis=1, keepdims=True)), 1.0)
             readout = numer / denom
             normed = readout * lax.rsqrt(
@@ -371,7 +386,7 @@
             normed = normed * head_buf[b : b + 1, lanes]
             gate = 1.0 / (1.0 + jnp.exp(-outgate[:, lanes]))
             gated_all[b, own, lanes] = (gate * normed).astype(BF16)
-        aux_out[b] = aux
+        keep_buf[...] = aux
 
         spread = []
         for k in range(1, ndp):
@@ -403,6 +418,7 @@
             )
             copy.start()
             outs.append(copy)
+        update_cells(b)
         if b + 1 < blocks:
             split_cells(b + 1)
         for c in outs:
@@ -418,29 +434,20 @@
             c.wait_send()
 
 
-def update_kernel(
-    cell, value, key, aux, normer, stab_in, rows_in, cell_out, normer_out, stab_out, rows_out
-):
-    chunk, heads, dh = cell.shape[1], cell.shape[2], cell.shape[3]
-    b = pl.program_id(0)
-    here = row_block(pl.program_id(1), chunk)
-    keep = aux[b, here, :]
-    for h in range(heads):
-        lanes = slice(h * dh, (h + 1) * dh)
-        across = jnp.transpose(value[b, here, lanes])
-        keys = key[b, here, lanes]
-        for j in range(chunk):
-            cell_out[0, j, h] = (
-                keep[j : j + 1, h : h + 1] * cell[0, j, h]
-                + across[:, j : j + 1] * keys[j : j + 1, :]
-            )
-        normer_out[0, :, h, :] = normer[b, here, lanes]
-    stab_out[...] = stab_in[...]
-    rows_out[...] = rows_in[...]
-
-
-def origin(ndim, b, c):
-    return (0,) * ndim
+def store_kernel(*refs):
+    sems = refs[-1]
+    half = (len(refs) - 1) // 2
+    copies = [
+        pltpu.make_async_copy(refs[i], refs[half + i], sems.at[i]) for i in range(half)
+    ]
+    for c in copies:
+        c.start()
+    for c in copies:
+        c.wait()
+
+
+def kernel_grant(*kept):
+    return 67_043_328 - sum(a.size * a.dtype.itemsize for a in kept) - 65536
 
 
 def per_device(ntp, ndp, *args):
@@ -455,33 +462,34 @@
     wig, wfg, stab = (jnp.swapaxes(a, 1, 2) for a in (wig, wfg, stab))
     batch = rows * ntp
     lanes = -(-(2 * all_heads + 1) // 128) * 128
+    vmem = pl.BlockSpec(memory_space=pltpu.VMEM)
     hbm = pl.BlockSpec(memory_space=pltpu.HBM)
     dma = pltpu.SemaphoreType.DMA
-    final_rows, value, key, normer_rows, aux, stab_rows = pl.pallas_call(
+    results = pl.pallas_call(
         functools.partial(step_kernel, ntp, ndp),
         out_shape=(
             jax.ShapeDtypeStruct(tokens.shape, BF16),
-            jax.ShapeDtypeStruct((blocks, seqs, inner), F32),
-            jax.ShapeDtypeStruct((blocks, seqs, inner), F32),
-            jax.ShapeDtypeStruct((blocks, seqs, inner), F32),
-            jax.ShapeDtypeStruct((blocks, seqs, lanes), F32),
+            jax.ShapeDtypeStruct(cell.shape, F32),
+            jax.ShapeDtypeStruct(normer.shape, F32),
             jax.ShapeDtypeStruct(stab.shape, F32),
         ),
         in_specs=[hbm] * 13,
-        out_specs=(pl.BlockSpec(),) * 6,
+        out_specs=(vmem,) * 4,
         scratch_shapes=[
             pltpu.VMEM((blocks, 4, width, inner), BF16),
             pltpu.VMEM((blocks, all_heads, width), BF16),
             pltpu.VMEM((blocks, all_heads, width), BF16),
             pltpu.VMEM(proj.shape, BF16),
-            pltpu.VMEM(cell.shape, F32),
+            pltpu.VMEM((seqs, inner), F32),
+            pltpu.VMEM((seqs, inner), F32),
+            pltpu.VMEM((seqs, lanes), F32),
             dma,
             dma((4,)),
             pltpu.VMEM(norm_gain.shape, F32),
             pltpu.VMEM(head_gain.shape, F32),
             pltpu.VMEM(normer.shape, F32),
             pltpu.VMEM(stab.shape, F32),
-            pltpu.VMEM((seqs, heads, dh, 2 * dh), BF16),
+            pltpu.VMEM((heads, seqs * dh, 2 * dh), BF16),
             pltpu.VMEM((blocks, batch, width), BF16),
             pltpu.VMEM((blocks, batch, 4 * inner), F32),
             pltpu.VMEM((blocks, batch, lanes), F32),
@@ -491,8 +499,6 @@
             pltpu.VMEM((blocks, more, seqs, lanes), F32),
             pltpu.VMEM((blocks, more, seqs, 4 * inner), F32),
             pltpu.VMEM((blocks, more, seqs, lanes), F32),
-            pltpu.VMEM((seqs, inner), F32),
-            pltpu.VMEM((seqs, inner), F32),
             pltpu.VMEM((blocks, batch, inner), BF16),
             pltpu.VMEM((batch, width), F32),
             pltpu.VMEM((blocks, batch, width), BF16),
@@ -515,35 +521,18 @@
             dma((blocks, ntp - 1)),
         ],
         compiler_params=pltpu.CompilerParams(
-            collective_id=0, has_side_effects=True, vmem_limit_bytes=67_043_328
+            collective_id=0, has_side_effects=True, vmem_limit_bytes=kernel_grant(cell, normer, tokens)
         ),
     )(tokens, wq, wk, wv, wo, wig, wfg, norm_gain, head_gain, proj, cell, normer, stab)
 
-    chunk = math.gcd(seqs, 8)
-    whole_rows = pl.BlockSpec(tokens.shape, lambda b, c: (0, 0))
-    whole_stab = pl.BlockSpec(stab.shape, lambda b, c: (0, 0, 0))
-    cell_spec = pl.BlockSpec((1, chunk, heads, dh, dh), lambda b, c: (b, c, 0, 0, 0))
-    cell_out, normer_out, stab_out, rows_out = pl.pallas_call(
-        update_kernel,
-        grid=(blocks, seqs // chunk),
-        out_shape=(
-            jax.ShapeDtypeStruct(cell.shape, F32),
-            jax.ShapeDtypeStruct(normer.shape, F32),
-            jax.ShapeDtypeStruct(stab.shape, F32),
-            jax.ShapeDtypeStruct(tokens.shape, BF16),
-        ),
-        in_specs=[cell_spec]
-        + [
-            pl.BlockSpec(a.shape, functools.partial(origin, a.ndim))
-            for a in (value, key, aux, normer_rows, stab_rows, final_rows)
-        ],
-        out_specs=(
-            cell_spec,
-            pl.BlockSpec((1, chunk, heads, dh), lambda b, c: (b, c, 0, 0)),
-            whole_stab,
-            whole_rows,
-        ),
-    )(cell, value, key, aux, normer_rows, stab_rows, final_rows)
+    shapes = tuple(jax.ShapeDtypeStruct(a.shape, a.dtype) for a in results)
+    rows_out, cell_out, normer_out, stab_out = pl.pallas_call(
+        store_kernel,
+        out_shape=shapes,
+        in_specs=[vmem] * 4,
+        out_specs=(hbm,) * 4,
+        scratch_shapes=[dma((4,))],
+    )(*results)
     return rows_out, cell_out, normer_out, jnp.swapaxes(stab_out, 1, 2)
 
 

time: 71 us -> 68.4 us (0.963)
  Pallas kernels: 70.1 us -> 67.6 us
    pallas_call x1, Pallas kernels: 10.7 us -> 6.83 us  [per_device(): pl.pallas_call(store_kernel, out_shape=shapes, in_specs=[vmem] * 4, out_s...]
    pallas_call x1, Pallas kernels: 59.4 us -> 60.8 us  [per_device(): pl.pallas_call(functools.partial(step_kernel, ntp, ndp), out_shape=(jax.S...]
where the time goes in v2:
time: 68.4 us; the launch traced here: 68.3 us
  Pallas kernels  67.6 us (99%)
    pallas_call x1, Pallas kernels, per_device(): pl.pallas_call(functools.partial(step_kernel, ntp, ndp), out_shape=(jax.S...  60.8 us
    pallas_call x1, Pallas kernels, per_device(): pl.pallas_call(store_kernel, out_shape=shapes, in_specs=[vmem] * 4, out_s...  6.83 us

profile of v2, /device:TPU:0, one launch (start us, length us, event | category | flops | bytes accessed | tf_op | source)
XLA Modules:
  0.0 68.3 jit_solution(435649449838189762)
XLA Ops:
  0.6 60.8 %shard_map.156 = (bf16[16,1024]{1,0:T(8,128)(2,1)}, f32[2,32,2,128,128]{4,3,2,1,0:T(8,128)}, f32[2,32,2,128]{3,2,1,0:T(2,128)}, f32[2,2,32]{2,1,0:T(2,128)}) custom-call(bf16[16,1024]{1,0:T(8,128)(2,1)} %tokens.1, bf16[2,1024,256]{2,1,0:T(8,128)(2,1)} %wq.1, bf16[2,1024,256]{2,1,0:T(8,128)(2,1)} %wk.1, bf16[2,1024,256]{2,1,0:T(8,128)(2,1)} %wv.1, ...), custom_call_target="tpu_custom_call" | custom-call | tf_op jit(solution)/shard_map/pallas_call | solution.py:468
  61.4 6.8 %shard_map.157 = (bf16[16,1024]{1,0:T(8,128)(2,1)}, f32[2,32,2,128,128]{4,3,2,1,0:T(8,128)}, f32[2,32,2,128]{3,2,1,0:T(2,128)}, f32[2,2,32]{2,1,0:T(2,128)}) custom-call(bf16[16,1024]{1,0:T(8,128)(2,1)} %get-tuple-element.12.refs_0_, f32[2,32,2,128,128]{4,3,2,1,0:T(8,128)} %get-tuple-element.13.refs_1_, f32[2,32,2,128]{3,2,1,0:T(2,128)} %get-tuple-element.14.refs_2_, ...), custom_call_target="tpu_custom_call" | custom-call | tf_op jit(solution)/shard_map/pallas_call | solution.py:529
